TPU v7x, 32 devices: a whole 2x2x4 slice. The times are simulated.
32 devices in a mesh: sp: 8 (over z, y), tp: 4 (over x, core).
Axes of the slice: x: 2, y: 2, z: 4, core: 2. Of those that a mesh axis runs over, the one named last changes fastest.
Arguments:
- prompt: bfloat16 [4, 1536, 4096], P(None, 'sp'), may hold values from -6 to 6
- forget_weight: bfloat16 [4096, 2048], P(None, 'tp'), may hold values from -0.09375 to 0.09375
- value_weight: bfloat16 [4096, 2048], P(None, 'tp'), may hold values from -1.5 to 1.5
- lower_bound: float32 [2048], P('tp'), may hold values from 0.9 to 0.9996745
- extra_decay: float32 [4, 1536, 2048], P(None, 'sp', 'tp'), may hold values from -1.4045573 to 0
- new_token: bfloat16 [4, 4096], P(None, 'tp'), may hold values from -6 to 6
- new_query: bfloat16 [4, 2048], P(None, 'tp'), may hold values from -6 to 6
- read_gain: float32 [128], replicated, may hold values from 0.1 to 1.9
Outputs:
- state_cache: bfloat16 [128, 16, 4, 128], P('sp', 'tp')
- first_read: bfloat16 [4, 2048], P(None, 'tp')
All inputs are finite; a program needn't handle non-finite values.
Results may differ from a plain program's by a relative error of at most 0.0019.
The roundings to bfloat16 on the way count: a program that leaves them out, or rounds other values in their place, can miss the bound.
Values may be sent and summed in bfloat16 or wider, within the bound.
A program may use at most 64 MiB of HBM per device.

v0:
```python
import jax
import jax.numpy as jnp
from jax import lax
from jax.sharding import PartitionSpec as P

HD = 128


def entering(value, axis, join, neutral):
    count, mine = (lax.axis_size(axis), lax.axis_index(axis))
    pieces = lax.all_gather(value, axis)
    pieces = pieces[::-1]
    mine = count - 1 - mine
    total = jnp.full_like(value, 0) + jnp.asarray(neutral, value.dtype)

    def hop(position, total):
        longer = join(total, pieces[position])
        return jnp.where(position < mine, longer, total)

    return lax.fori_loop(0, count - 1, hop, total)


def add_terms(earlier, latter):
    return earlier + latter


def read_share(state_rows, decay_rows, key_share, query_rows, new_value):
    updated = jnp.exp(decay_rows)[..., None] * state_rows + key_share[..., None] * new_value[None]
    return jnp.sum(query_rows[..., None] * updated, axis=0)


def local(
    prompt, forget_weight, value_weight, lower_bound, extra_decay, new_token, new_query, read_gain
):
    seq_count = prompt.shape[0]
    span_len = prompt.shape[1]
    width_dev = forget_weight.shape[1]
    head_count = width_dev // HD
    log_lower = jnp.log(lower_bound)
    log_upper = jnp.log1p(-lower_bound)
    opening = 1.0 - lower_bound
    forget_pre = jnp.einsum(
        "std,dw->stw", prompt, forget_weight, preferred_element_type=jnp.float32
    ).astype(jnp.bfloat16)
    values = jnp.einsum(
        "std,dw->stw", prompt, value_weight, preferred_element_type=jnp.float32
    ).astype(jnp.bfloat16)
    forget_wide = lax.optimization_barrier(forget_pre).astype(jnp.float32)
    log_forget = jnp.logaddexp(log_lower, log_upper + jax.nn.log_sigmoid(forget_wide)) + extra_decay
    key_rows = opening * jax.nn.sigmoid(-forget_wide)
    running = jnp.cumsum(log_forget, axis=1)
    totals = running[:, -1]
    weighted = (key_rows * jnp.exp(totals[:, None] - running)).astype(jnp.bfloat16)
    weighted = weighted.reshape(seq_count, span_len, head_count, HD)
    value_rows = values.reshape(seq_count, span_len, head_count, HD)
    later_sum = entering(totals, "sp", add_terms, jnp.zeros_like(totals))
    end_scale = jnp.exp(later_sum).reshape(seq_count, head_count, HD).transpose(2, 1, 0)
    whole_token = lax.all_gather(new_token, "tp", axis=1, tiled=True)
    new_forget = lax.optimization_barrier(
        jnp.dot(whole_token, forget_weight, preferred_element_type=jnp.float32).astype(jnp.bfloat16)
    ).astype(jnp.float32)
    new_value = lax.optimization_barrier(
        jnp.dot(whole_token, value_weight, preferred_element_type=jnp.float32).astype(jnp.bfloat16)
    ).astype(jnp.float32)
    new_log = jnp.logaddexp(log_lower, log_upper + jax.nn.log_sigmoid(new_forget))
    new_key = opening * jax.nn.sigmoid(-new_forget)
    query_act = jax.nn.silu(new_query.astype(jnp.float32))
    decay_cols = new_log.reshape(seq_count, head_count, HD).transpose(2, 1, 0)
    key_cols = new_key.reshape(seq_count, head_count, HD).transpose(2, 1, 0)
    query_cols = query_act.reshape(seq_count, head_count, HD).transpose(2, 1, 0)
    value_cols = new_value.reshape(seq_count, head_count, HD).transpose(1, 0, 2)
    row_share = HD // lax.axis_size("sp")
    first_own = lax.axis_index("sp") * row_share
    block_state = jnp.einsum(
        "sthd,sthe->dhse", weighted, value_rows, preferred_element_type=jnp.float32
    )
    whole_state = lax.psum(block_state * end_scale[..., None], "sp")
    state_cache = lax.dynamic_slice_in_dim(whole_state, first_own, row_share, 0).astype(
        jnp.bfloat16
    )
    raw_read = read_share(whole_state, decay_cols, key_cols, query_cols, value_cols)
    raw_read = raw_read.transpose(1, 0, 2)
    normed = (
        raw_read
        * lax.rsqrt(jnp.mean(raw_read * raw_read, axis=-1, keepdims=True) + 1e-06)
        * read_gain
    )
    first_read = normed.reshape(seq_count, width_dev).astype(jnp.bfloat16)
    return (state_cache, first_read)


def solution(mesh):
    return jax.shard_map(
        local,
        mesh=mesh,
        in_specs=(
            P(None, "sp", None),
            P(None, "tp"),
            P(None, "tp"),
            P("tp"),
            P(None, "sp", "tp"),
            P(None, "tp"),
            P(None, "tp"),
            P(),
        ),
        out_specs=(P("sp", "tp", None, None), P(None, "tp")),
        check_vma=False,
    )
```

profile of v0, /device:TPU:0, one launch (start us, length us, event | category | flops | bytes accessed | tf_op | source)
XLA Modules:
  0.0 154.1 jit_solution(2838277091920605518)
XLA Ops:
  7.2 0.7 broadcast_subtract_fusion
  7.9 7.5 %fusion.23 = bf16[4,192,512]{2,1,0:T(8,128)(2,1)S(1)} fusion(bf16[4,192,4096]{2,1,0:T(8,128)(2,1)} %param.10, bf16[4096,512]{1,0:T(8,128)(2,1)} %param.11), kind=kOutput, calls=%fused_computation.27 | convolution fusion | flops 3221618688 | bytes 11272192 | tf_op jit(solution)/shard_map/std,dw->stw/dot_general | solution.py:42
  15.5 2.0 %add_bitcast_fusion = f32[4,512,192]{1,2,0:T(8,128)S(1)} fusion(f32[4,192,512]{2,1,0:T(8,128)S(1)} %copy-done.1, bf16[4,192,512]{2,1,0:T(8,128)(2,1)S(1)} %fusion.23, f32[512]{0:T(512)S(1)} %get-tuple-element.112, f32[512]{0:T(512)S(1)} %get-tuple-element.113), kind=kLoop, calls=%fused_computation.24 | loop fusion | flops 7471104 | bytes 3936256 | tf_op jit(solution)/shard_map/transpose
  17.4 0.2 pad.3
  17.7 1.6 %fusion.4 = f32[4,512,2,128]{1,2,3,0:T(2,128)S(1)} fusion(f32[4,512,2,128]{1,3,2,0:T(8,128)S(1)} %bitcast.83), kind=kOutput, calls=%fused_computation.6 | output fusion | flops 66584576 | bytes 4194304 | tf_op jit(solution)/shard_map/reduce-window
  19.3 0.1 reduce-window.9
  19.4 0.7 broadcast_add_fusion
  20.1 0.4 copy.21
  20.6 32.4 %all-gather = f32[32,1,512]{2,1,0:T(1,128)S(1)} all-gather(f32[4,1,512]{2,1,0:T(1,128)S(1)} %slice.19), channel_id=2, replica_groups=mesh['sp'=8,'tp'=4] {'sp'}, dimensions={0}, use_global_device_ids=true | all-gather | bytes 73728 | tf_op jit(solution)/shard_map/all_gather | solution.py:11
  52.9 0.2 reduce
  53.1 0.3 while.14
  53.4 7.4 %fusion.27 = bf16[4,24,4,8,128]{4,3,2,1,0:T(8,128)(2,1)S(1)} fusion(bf16[4,192,4096]{2,1,0:T(8,128)(2,1)} %param.10, bf16[4096,512]{1,0:T(8,128)(2,1)} %param.12), kind=kOutput, calls=%fused_computation.30 | convolution fusion | flops 3221618688 | bytes 11272192 | tf_op jit(solution)/shard_map/std,dw->stw/dot_general | solution.py:45
  60.9 2.0 %fusion.26 = f32[128,4,4,128]{0,3,2,1:T(8,128)} fusion(bf16[4,24,4,8,128]{4,3,2,1,0:T(8,128)(2,1)S(1)} %fusion.27, f32[128,4,4]{0,2,1:T(4,128)S(1)} %exponential_bitcast_fusion.1, f32[4,256,512]{2,1,0:T(8,128)S(1)} %bitcast.85, f32[4,512]{1,0:T(4,128)S(1)} %bitcast.86, bf16[4,192,512]{2,1,0:T(8,128)(2,1)S(1)} %fusion.23, f32[512]{0:T(512)S(1)} %get-tuple-element.111), kind=kOutput, calls=%fused_computation.29 | convolution fusion | flops 103677952 | bytes 4212736 | tf_op jit(solution)/shard_map/sthd,sthe->dhse/dot_general | solution.py:74
  62.9 5.2 %all_gather.7 = bf16[4,4096]{1,0:T(4,128)(2,1)S(1)} all-gather(bf16[4,1024]{1,0:T(4,128)(2,1)S(1)} %copy-done.2), channel_id=1, replica_groups=mesh['sp'=8,'tp'=4] {'tp'}, dimensions={1}, use_global_device_ids=true | all-gather | bytes 40960 | tf_op jit(solution)/shard_map/all_gather | solution.py:58
  68.1 3.2 %convolution_convert_fusion.1 = bf16[4,512]{1,0:T(4,128)(2,1)S(1)} fusion(bf16[4,4096]{1,0:T(4,128)(2,1)S(1)} %all_gather.7, bf16[4096,512]{1,0:T(8,128)(2,1)} %param.11), kind=kOutput, calls=%fused_computation.32 | convolution fusion | flops 16779264 | bytes 4231168 | tf_op jit(solution)/shard_map/dot_general | solution.py:60
  71.4 0.5 copy-done
  71.8 0.6 convolution_convert_fusion
  72.5 0.1 exponential_bitcast_fusion
  72.6 69.7 %all-reduce.3.cloned.1.call-done = f32[128,4,4,128]{0,3,2,1:T(8,128)} async-done(((f32[128,4,4,128]{0,3,2,1:T(8,128)}), f32[128,4,4,128]{0,3,2,1:T(8,128)}) %all-reduce.3.cloned.1.call-update) | async-done | bytes 1048592 | tf_op jit(solution)/shard_map/psum | solution.py:77
  142.3 1.9 %multiply_reduce_fusion = f32[4,4,128]{2,1,0:T(4,128)S(1)} fusion(f32[128,4,4,128]{0,3,2,1:T(8,128)} %all-reduce.3.cloned.1.call-done, f32[4,4,128]{2,1,0:T(4,128)S(1)} %convert_bitcast_fusion, f32[128,4,4]{0,2,1:T(4,128)S(1)} %get-tuple-element.110, f32[128,4,4]{0,2,1:T(4,128)S(1)} %get-tuple-element.109, f32[128,4,4]{0,2,1:T(4,128)S(1)} %get-tuple-element.114), kind=kLoop, calls=%fused_computation.33 | loop fusion | flops 1308672 | bytes 1089536 | tf_op jit(solution)/shard_map/reduce_sum | solution.py:29
  144.2 0.1 fusion.50
  144.3 1.4 dynamic-slice_convert_fusion
  145.7 0.8 copy.29
  146.6 0.7 fusion.53
  (28 shorter events, 0.3 us)
Async XLA Ops:
  7.2 135.2 %all-reduce.3.cloned.1.call-start = ((), (), s32[]{:S(2)}) async-start(), calls=%async_computation | async-start | bytes 2097152 | tf_op jit(solution)/shard_map/psum | solution.py:77
  7.9 7.5 %copy-start.1 = (f32[4,192,512]{2,1,0:T(8,128)S(1)}, f32[4,192,512]{2,1,0:T(8,128)}, u32[]{:S(2)}) copy-start(f32[4,192,512]{2,1,0:T(8,128)} %param.14) | copy-start | bytes 4718596
  60.9 2.1 %copy-start.2 = (bf16[4,1024]{1,0:T(4,128)(2,1)S(1)}, bf16[4,1024]{1,0:T(4,128)(2,1)}, u32[]{:S(2)}) copy-start(bf16[4,1024]{1,0:T(4,128)(2,1)} %param.15) | copy-start | bytes 24580
  68.1 3.7 %copy-start = (bf16[4096,512]{1,0:T(8,128)(2,1)S(1)}, bf16[4096,512]{1,0:T(8,128)(2,1)}, u32[]{:S(2)}) copy-start(bf16[4096,512]{1,0:T(8,128)(2,1)} %param.12) | copy-start | bytes 12582916
  71.8 0.7 copy-start.3
  72.5 74.1 %copy-start.4 = (f32[128]{0:T(128)S(1)}, f32[128]{0:T(128)}, u32[]{:S(2)}) copy-start(f32[128]{0:T(128)} %param.17) | copy-start | bytes 1540
Sparse Core Ops, SparseCore 0:
  63.0 79.2 all-reduce.2
where the time goes:
time: 154 us
  waiting for transfers between devices  69.8 us (45%)
  blocking collectives  37.5 us (24%)
  matrix products  20.8 us (14%)
  between operations  14.2 us (9%)
  other arithmetic  8.07 us (5%)
  local copies, waits for them, and re-layouts  3.48 us (2%)
    psum x1, waiting for transfers between devices, local(): whole_state = lax.psum(block_state * end_scale[..., None], 'sp')  69.7 us
    all_gather x1, blocking collectives, entering(): pieces = lax.all_gather(value, axis)  32.4 us
    dot_general x1, matrix products, local(): jnp.einsum('std,dw->stw', prompt, forget_weight, preferred_element_type=j...  7.52 us
    dot_general x1, matrix products, local(): jnp.einsum('std,dw->stw', prompt, value_weight, preferred_element_type=jn...  7.42 us
    all_gather x1, blocking collectives, local(): whole_token = lax.all_gather(new_token, 'tp', axis=1, tiled=True)  5.19 us
    dot_general x1, matrix products, local(): jnp.dot(whole_token, forget_weight, preferred_element_type=jnp.float32)  3.23 us
  transfers between devices with their start and end apart: 1, of which 1 were waited for; matrix products, arithmetic and copies ran while one was open for 3% of the time, Pallas kernels for 0%

commit v1 on v0

--- a/solution.py
+++ b/solution.py
@@ -1,9 +1,18 @@
+import functools
 import jax
 import jax.numpy as jnp
 from jax import lax
 from jax.sharding import PartitionSpec as P
 
 HD = 128
+
+
+def numbers_process(a0, axis_name):
+    response = lax.all_gather(a0, axis_name=axis_name).sum(axis=0)
+    return response
+
+
+quarters_pack = functools.partial(numbers_process, axis_name="sp")
 
 
 def entering(value, axis, join, neutral):
@@ -74,7 +83,7 @@
     block_state = jnp.einsum(
         "sthd,sthe->dhse", weighted, value_rows, preferred_element_type=jnp.float32
     )
-    whole_state = lax.psum(block_state * end_scale[..., None], "sp")
+    whole_state = quarters_pack(block_state * end_scale[..., None])
     state_cache = lax.dynamic_slice_in_dim(whole_state, first_own, row_share, 0).astype(
         jnp.bfloat16
     )

time: 154 us -> 213 us (1.38)
  waiting for transfers between devices: 69.8 us -> 114 us
  local copies, waits for them, and re-layouts: 3.48 us -> 10.5 us
  other arithmetic: 8.07 us -> 12.6 us
  matrix products: 20.8 us -> 23.1 us
    all_gather x0 -> x1, waiting for transfers between devices: none -> 114 us  [numbers_process(): response = lax.all_gather(a0, axis_name=axis_name).sum(axis=0)]
    psum x1 -> x0, waiting for transfers between devices: 69.7 us -> none  [local(): whole_state = lax.psum(block_state * end_scale[..., None], 'sp')]
    unnamed x12 -> x11, local copies, waits for them, and re-layouts: 1.36 us -> 9.54 us
    reduce_sum x0 -> x1, other arithmetic: none -> 5.61 us  [numbers_process(): response = lax.all_gather(a0, axis_name=axis_name).sum(axis=0)]
    dot_general x1, matrix products: 0.64 us -> 3.26 us  [local(): jnp.dot(whole_token, value_weight, preferred_element_type=jnp.float32)]
where the time goes in v1:
time: 213 us
  waiting for transfers between devices  114 us (54%)
  blocking collectives  37.7 us (18%)
  matrix products  23.1 us (11%)
  between operations  14.2 us (7%)
  other arithmetic  12.6 us (6%)
  local copies, waits for them, and re-layouts  10.5 us (5%)
    all_gather x1, waiting for transfers between devices, numbers_process(): response = lax.all_gather(a0, axis_name=axis_name).sum(axis=0)  114 us
    all_gather x1, blocking collectives, entering(): pieces = lax.all_gather(value, axis)  32.4 us
    unnamed x11, local copies, waits for them, and re-layouts  9.54 us
    dot_general x1, matrix products, local(): jnp.einsum('std,dw->stw', prompt, forget_weight, preferred_element_type=j...  7.52 us
    dot_general x1, matrix products, local(): jnp.einsum('std,dw->stw', prompt, value_weight, preferred_element_type=jn...  7.41 us
    reduce_sum x1, other arithmetic, numbers_process(): response = lax.all_gather(a0, axis_name=axis_name).sum(axis=0)  5.61 us
    all_gather x1, blocking collectives, local(): whole_token = lax.all_gather(new_token, 'tp', axis=1, tiled=True)  5.37 us
  transfers between devices with their start and end apart: 1, of which 1 were waited for; matrix products, arithmetic and copies ran while one was open for 3% of the time, Pallas kernels for 0%

profile of v1, /device:TPU:0, one launch (start us, length us, event | category | flops | bytes accessed | tf_op | source)
XLA Modules:
  0.0 212.7 jit_solution(17090082848711890020)
XLA Ops:
  7.2 0.7 broadcast_subtract_fusion
  7.9 7.5 %fusion.23 = bf16[4,192,512]{2,1,0:T(8,128)(2,1)S(1)} fusion(bf16[4,192,4096]{2,1,0:T(8,128)(2,1)} %param.10, bf16[4096,512]{1,0:T(8,128)(2,1)} %param.11), kind=kOutput, calls=%fused_computation.27 | convolution fusion | flops 3221618688 | bytes 11272192 | tf_op jit(solution)/shard_map/std,dw->stw/dot_general | solution.py:51
  15.4 2.0 add_bitcast_fusion
  17.4 0.2 pad.3
  17.7 1.6 fusion.4
  19.4 0.7 broadcast_add_fusion
  20.1 0.4 copy.20
  20.5 32.4 %all-gather = f32[32,1,512]{2,1,0:T(1,128)S(1)} all-gather(f32[4,1,512]{2,1,0:T(1,128)S(1)} %slice.19), channel_id=2, replica_groups=mesh['sp'=8,'tp'=4] {'sp'}, dimensions={0}, use_global_device_ids=true | all-gather | bytes 73728 | tf_op jit(solution)/shard_map/all_gather | solution.py:20
  52.9 0.2 reduce
  53.1 0.3 while.14
  53.4 7.4 %fusion.27 = bf16[4,24,4,8,128]{4,3,2,1,0:T(8,128)(2,1)S(1)} fusion(bf16[4,192,4096]{2,1,0:T(8,128)(2,1)} %param.10, bf16[4096,512]{1,0:T(8,128)(2,1)} %param.12), kind=kOutput, calls=%fused_computation.30 | convolution fusion | flops 3221618688 | bytes 11272192 | tf_op jit(solution)/shard_map/std,dw->stw/dot_general | solution.py:54
  60.9 2.1 fusion.26
  63.0 5.4 %all_gather.15 = bf16[4,4096]{1,0:T(4,128)(2,1)S(1)} all-gather(bf16[4,1024]{1,0:T(4,128)(2,1)S(1)} %copy-done.1), channel_id=1, replica_groups=mesh['sp'=8,'tp'=4] {'tp'}, dimensions={1}, use_global_device_ids=true | all-gather | bytes 40960 | tf_op jit(solution)/shard_map/all_gather | solution.py:67
  68.3 2.8 %convolution_convert_fusion.1 = bf16[4,512]{1,0:T(4,128)(2,1)S(1)} fusion(bf16[4,4096]{1,0:T(4,128)(2,1)S(1)} %all_gather.15, bf16[4096,512]{1,0:T(8,128)(2,1)} %param.11), kind=kOutput, calls=%fused_computation.32 | convolution fusion | flops 16779264 | bytes 4231168 | tf_op jit(solution)/shard_map/dot_general | solution.py:69
  71.2 0.1 select_exponential_fusion
  71.3 3.3 %convolution_convert_fusion = bf16[4,512]{1,0:T(4,128)(2,1)S(1)} fusion(bf16[4,4096]{1,0:T(4,128)(2,1)S(1)} %all_gather.15, bf16[4096,512]{1,0:T(8,128)(2,1)} %param.12), kind=kOutput, calls=%fused_computation.31 | convolution fusion | flops 16779264 | bytes 4231168 | tf_op jit(solution)/shard_map/dot_general | solution.py:72
  74.6 114.3 %all-gather.4.cloned.1.call-done = f32[1024,4,4,128]{0,3,2,1:T(8,128)} async-done(((f32[128,4,4,128]{0,3,2,1:T(8,128)}), f32[1024,4,4,128]{0,3,2,1:T(8,128)}) %all-gather.4.cloned.1.call-update) | async-done | bytes 8388624 | tf_op jit(solution)/shard_map/all_gather | solution.py:11
  188.9 8.7 %copy.35 = f32[256,8,8,128]{3,2,1,0:T(8,128)} copy(f32[256,8,8,128]{3,1,2,0:T(8,128)} %bitcast.78) | data formatting | bytes 16777216
  197.6 5.6 %reduce_sum.27 = f32[128,4,4,128]{0,3,2,1:T(8,128)S(1)} reduce(f32[8,128,4,4,128]{1,0,4,3,2:T(8,128)} %bitcast.77, f32[]{:T(128)} %constant.50.clone.1), dimensions={0}, to_apply=%region_4.5 | reduce | flops 1835008 | bytes 9437188 | tf_op jit(solution)/shard_map/reduce_sum | solution.py:11
  203.2 0.7 multiply_reduce_fusion
  204.0 0.1 fusion.48
  204.1 0.2 dynamic-slice_convert_fusion
  204.3 0.8 copy.29
  205.1 0.7 fusion.51
  (36 shorter events, 0.4 us)
Async XLA Ops:
  7.2 181.8 %all-gather.4.cloned.1.call-start = ((), (), s32[]{:S(2)}) async-start(), calls=%async_computation | async-start | bytes 9437184 | tf_op jit(solution)/shard_map/all_gather | solution.py:11
  7.9 7.5 %copy-start = (f32[4,192,512]{2,1,0:T(8,128)S(1)}, f32[4,192,512]{2,1,0:T(8,128)}, u32[]{:S(2)}) copy-start(f32[4,192,512]{2,1,0:T(8,128)} %param.14) | copy-start | bytes 4718596
  60.8 2.1 copy-start.1
  71.3 3.3 %copy-start.2 = (bf16[4,512]{1,0:T(4,128)(2,1)S(1)}, bf16[4,512]{1,0:T(4,128)(2,1)}, u32[]{:S(2)}) copy-start(bf16[4,512]{1,0:T(4,128)(2,1)} %param.16) | copy-start | bytes 12292
  203.2 1.9 copy-start.3
Sparse Core Ops, SparseCore 0:
  63.1 125.8 all-gather.3
